TPU v7x, 32 devices: a whole 2x2x4 slice. The times are simulated.
32 devices in a mesh: kv: 8 (over z, x), tp: 4 (over y, core).
Axes of the slice: x: 2, y: 2, z: 4, core: 2. Of those that a mesh axis runs over, the one named last changes fastest.
Arguments:
- tokens: bfloat16 [16384, 2048], P('kv'), may hold values from -6 to 6
- norm_gain: bfloat16 [2048], replicated, may hold values from 0.099609375 to 1.8984375
- query_weight: bfloat16 [2048, 1024], P(None, 'tp'), may hold values from -0.125 to 0.125
- cmp_key_weight: bfloat16 [2048, 512], P(None, 'tp'), may hold values from -0.125 to 0.125
- cmp_value_weight: bfloat16 [2048, 512], P(None, 'tp'), may hold values from -0.125 to 0.125
- sel_key_weight: bfloat16 [2048, 512], P(None, 'tp'), may hold values from -0.125 to 0.125
- sel_value_weight: bfloat16 [2048, 512], P(None, 'tp'), may hold values from -0.125 to 0.125
- branch_weight: bfloat16 [2, 2048, 16], replicated, may hold values from -0.125 to 0.125
- key_embed: bfloat16 [8, 32, 64], P('tp'), may hold values from -3 to 3
- key_inner: bfloat16 [8, 2048, 64], P('tp'), may hold values from -0.125 to 0.125
- key_outer: bfloat16 [8, 64, 64], P('tp'), may hold values from -0.75 to 0.75
- value_embed: bfloat16 [8, 32, 64], P('tp'), may hold values from -3 to 3
- value_inner: bfloat16 [8, 2048, 64], P('tp'), may hold values from -0.125 to 0.125
- value_outer: bfloat16 [8, 64, 64], P('tp'), may hold values from -0.75 to 0.75
- out_weight: bfloat16 [1024, 2048], replicated, may hold values from -0.1875 to 0.1875
- chosen: int32 [8, 128, 8], P('tp'), may hold values from 0 to 255, as said below
Outputs:
- attended: bfloat16 [16384, 2048], P(('kv', 'tp'))
Inputs may be any that keep to these rules, and one draw needn't show every extreme that they name: `chosen`: each entry is the index of a block of 64 positions in the whole sequence. For every key head and query block, its 8 entries lie in 8 different aligned spans of 2048 positions (at most one from any span), and none lies inside the query block's own positions.
All inputs are finite; a program needn't handle non-finite values.
Results may differ from a plain program's by a relative error of at most 0.0075.
Values may be sent and summed in bfloat16 or wider, within the bound.
A program may use at most 128 MiB of HBM per device.

v0:
```python
import jax
import jax.numpy as jnp
from jax import lax
from jax.sharding import PartitionSpec as P

HEAD_DIM = 64
CMP_BLOCK = 32
SEL_BLOCK = 64
Q_BLOCK = 128
FAR_PICKS = 8
ROPE_BASE = 10000.0
norm_eps = 1e-06
masked_score = -1000000000.0


def rotate(values_in, positions):
    half_dim = values_in.shape[-1] // 2
    inverse = ROPE_BASE ** (-jnp.arange(half_dim, dtype=jnp.float32) / half_dim)
    rotary_phases = positions.astype(jnp.float32)[:, None] * inverse[None, :]
    cosine = jnp.cos(rotary_phases)[:, None, :]
    sine = jnp.sin(rotary_phases)[:, None, :]
    first_half = values_in[..., :half_dim]
    second_half = values_in[..., half_dim:]
    return jnp.concatenate(
        [first_half * cosine - second_half * sine, second_half * cosine + first_half * sine],
        axis=-1,
    )


def summarize(raw_rows, embed, inner, outer):
    kv_local = embed.shape[0]
    block_count = raw_rows.shape[0] // CMP_BLOCK
    blocked = (
        raw_rows.reshape(block_count, CMP_BLOCK, kv_local, HEAD_DIM)
        .transpose(2, 0, 1, 3)
        .astype(jnp.float32)
    )
    blocked = (blocked + embed.astype(jnp.float32)[:, None]).astype(jnp.bfloat16)
    blocked = blocked.reshape(kv_local, block_count, CMP_BLOCK * HEAD_DIM)
    hidden = jax.nn.gelu(
        jnp.einsum("knc,kce->kne", blocked, inner, preferred_element_type=jnp.float32)
    ).astype(jnp.bfloat16)
    return jnp.einsum("kne,kef->knf", hidden, outer, preferred_element_type=jnp.float32).astype(
        jnp.bfloat16
    )


def per_device(
    tokens,
    norm_gain,
    query_weight,
    cmp_key_weight,
    cmp_value_weight,
    sel_key_weight,
    sel_value_weight,
    branch_weight,
    key_embed,
    key_inner,
    key_outer,
    value_embed,
    value_inner,
    value_outer,
    out_weight,
    chosen,
):
    tok_rows = tokens.shape[0]
    kv_local = key_embed.shape[0]
    heads_local = query_weight.shape[1] // HEAD_DIM
    group_size = heads_local // kv_local
    owners = lax.axis_size("kv")
    dev_index = lax.axis_index("kv")
    offset = dev_index * tok_rows
    positions = offset + jnp.arange(tok_rows, dtype=jnp.int32)
    scale = HEAD_DIM ** (-0.5)
    expanded_mask = tokens.astype(jnp.float32)
    normed = (
        expanded_mask
        * lax.rsqrt(jnp.mean(expanded_mask * expanded_mask, axis=-1, keepdims=True) + norm_eps)
        * norm_gain.astype(jnp.float32)
    ).astype(jnp.bfloat16)
    gate_cols = lax.dynamic_slice_in_dim(
        branch_weight, lax.axis_index("tp") * heads_local, heads_local, 2
    )
    q_width = heads_local * HEAD_DIM
    kv_width = kv_local * HEAD_DIM
    joined_weight = jnp.concatenate(
        [
            query_weight,
            cmp_key_weight,
            cmp_value_weight,
            sel_key_weight,
            sel_value_weight,
            gate_cols[0],
            gate_cols[1],
        ],
        axis=1,
    )
    projected = jnp.dot(normed, joined_weight, preferred_element_type=jnp.float32)
    bounds = [
        q_width,
        q_width + kv_width,
        q_width + 2 * kv_width,
        q_width + 3 * kv_width,
        q_width + 4 * kv_width,
        q_width + 4 * kv_width + heads_local,
    ]
    (
        query_part,
        cmp_key_part,
        cmp_value_part,
        sel_key_part,
        sel_value_part,
        gate_cmp_part,
        gate_sel_part,
    ) = jnp.split(projected, bounds, axis=1)
    query = query_part.reshape(tok_rows, heads_local, HEAD_DIM)
    q_plain = query.astype(jnp.bfloat16)
    q_turn = rotate(query, positions).astype(jnp.bfloat16)
    cmp_key = cmp_key_part.astype(jnp.bfloat16).reshape(tok_rows, kv_local, HEAD_DIM)
    cmp_value = cmp_value_part.astype(jnp.bfloat16).reshape(tok_rows, kv_local, HEAD_DIM)
    sel_key = rotate(sel_key_part.reshape(tok_rows, kv_local, HEAD_DIM), positions).astype(
        jnp.bfloat16
    )
    selected_value = sel_value_part.astype(jnp.bfloat16).reshape(tok_rows, kv_local, HEAD_DIM)
    gate_cmp = jax.nn.sigmoid(gate_cmp_part)
    gate_sel = jax.nn.sigmoid(gate_sel_part)
    summary = jnp.concatenate(
        [
            summarize(cmp_key, key_embed, key_inner, key_outer),
            summarize(cmp_value, value_embed, value_inner, value_outer),
        ],
        axis=-1,
    )
    summaries = lax.all_gather(summary, "kv", axis=1, tiled=True)
    summary_count = summaries.shape[1]
    block_end = (jnp.arange(summary_count, dtype=jnp.int32) + 1) * CMP_BLOCK - 1
    q_group = q_plain.reshape(tok_rows, kv_local, group_size, HEAD_DIM).transpose(1, 0, 2, 3)
    cmp_scores = (
        jnp.einsum(
            "ktgd,kcd->ktgc", q_group, summaries[..., :HEAD_DIM], preferred_element_type=jnp.float32
        )
        * scale
    )
    usable = (block_end[None, :] <= positions[:, None])[None, :, None, :]
    cmp_probs = jax.nn.softmax(
        jnp.where(usable, cmp_scores, masked_score), axis=-1
    ) * usable.astype(jnp.float32)
    out_cmp = jnp.einsum(
        "ktgc,kcd->ktgd",
        cmp_probs.astype(jnp.bfloat16),
        summaries[..., HEAD_DIM:],
        preferred_element_type=jnp.float32,
    )
    out_cmp = out_cmp.transpose(1, 0, 2, 3).reshape(tok_rows, heads_local, HEAD_DIM)
    span_queries = tok_rows // Q_BLOCK
    kv_sel = jnp.concatenate([sel_key, selected_value], axis=-1).transpose(1, 0, 2)
    all_picks = chosen.reshape(kv_local, owners, span_queries, FAR_PICKS)
    my_picks = lax.dynamic_index_in_dim(all_picks, dev_index, 1, keepdims=False)
    head_lane = jnp.arange(kv_local, dtype=jnp.int32)[:, None, None]
    empty = jnp.zeros((kv_local, span_queries, FAR_PICKS, SEL_BLOCK, 2 * HEAD_DIM), jnp.bfloat16)
    piece = lax.all_gather(kv_sel, "kv", axis=1, tiled=True)
    block_count = piece.shape[1] // SEL_BLOCK
    blocked = piece.reshape(kv_local, block_count, SEL_BLOCK, 2 * HEAD_DIM)
    inside = (my_picks >= 0) & (my_picks < block_count)
    clipped = jnp.clip(my_picks, 0, block_count - 1)
    fetched = blocked[head_lane, clipped]
    picked = jnp.where(inside[..., None, None], fetched, empty)
    own_keys = kv_sel.reshape(kv_local, span_queries, Q_BLOCK, 2 * HEAD_DIM)
    keys_all = jnp.concatenate(
        [own_keys, picked.reshape(kv_local, span_queries, FAR_PICKS * SEL_BLOCK, 2 * HEAD_DIM)],
        axis=2,
    )
    query_pos = positions.reshape(span_queries, Q_BLOCK)
    far_pos = (my_picks[..., None] * SEL_BLOCK + jnp.arange(SEL_BLOCK, dtype=jnp.int32)).reshape(
        kv_local, span_queries, FAR_PICKS * SEL_BLOCK
    )
    key_pos = jnp.concatenate(
        [jnp.broadcast_to(query_pos[None], (kv_local, span_queries, Q_BLOCK)), far_pos], axis=2
    )
    q_sel = q_turn.reshape(span_queries, Q_BLOCK, kv_local, group_size, HEAD_DIM).transpose(
        2, 0, 1, 3, 4
    )
    sel_scores = (
        jnp.einsum(
            "knqgd,knmd->knqgm", q_sel, keys_all[..., :HEAD_DIM], preferred_element_type=jnp.float32
        )
        * scale
    )
    allowed_keys = key_pos[:, :, None, None, :] <= query_pos[None, :, :, None, None]
    sel_probs = jax.nn.softmax(jnp.where(allowed_keys, sel_scores, masked_score), axis=-1)
    out_sel = jnp.einsum(
        "knqgm,knmd->knqgd",
        sel_probs.astype(jnp.bfloat16),
        keys_all[..., HEAD_DIM:],
        preferred_element_type=jnp.float32,
    )
    out_sel = out_sel.transpose(1, 2, 0, 3, 4).reshape(tok_rows, heads_local, HEAD_DIM)
    mixed = (
        (gate_cmp[..., None] * out_cmp + gate_sel[..., None] * out_sel)
        .reshape(tok_rows, heads_local * HEAD_DIM)
        .astype(jnp.bfloat16)
    )
    head_rows = lax.all_to_all(mixed, "tp", split_axis=0, concat_axis=1, tiled=True)
    return jnp.dot(head_rows, out_weight, preferred_element_type=jnp.float32).astype(jnp.bfloat16)


def solution(mesh):
    placed = (
        P("kv", None),
        P(),
        P(None, "tp"),
        P(None, "tp"),
        P(None, "tp"),
        P(None, "tp"),
        P(None, "tp"),
        P(),
        P("tp", None, None),
        P("tp", None, None),
        P("tp", None, None),
        P("tp", None, None),
        P("tp", None, None),
        P("tp", None, None),
        P(),
        P("tp", None, None),
    )
    return jax.shard_map(
        per_device, mesh=mesh, in_specs=placed, out_specs=P(("kv", "tp"), None), check_vma=False
    )
```

profile of v0, /device:TPU:0, one launch (start us, length us, event | category | flops | bytes accessed | tf_op | source)
XLA Modules:
  0.0 275.9 jit_solution(4170866323818475863)
XLA Ops:
  6.6 0.7 convert_element_type.94
  7.3 5.1 %fusion.2 = f32[2048]{0:T(1024)S(1)} fusion(bf16[2048,2048]{1,0:T(8,128)(2,1)} %param.16), kind=kLoop, calls=%fused_computation.8 | loop fusion | flops 12580864 | bytes 8396800 | tf_op jit(solution)/shard_map/reduce_sum | solution.py:78
  12.4 0.9 dynamic-slice_bitcast_fusion
  13.3 0.3 copy.102
  13.6 0.3 copy.101
  13.9 1.0 multiply_cosine_fusion
  14.9 1.3 copy.114
  16.2 1.3 copy.116
  17.5 6.6 %concatenate.30 = bf16[2048,776]{1,0:T(8,128)(2,1)} concatenate(bf16[2048,256]{1,0:T(8,128)(2,1)S(1)} %copy-done.6, bf16[2048,128]{1,0:T(8,128)(2,1)} %param.19, bf16[2048,128]{1,0:T(8,128)(2,1)} %param.20, bf16[2048,128]{1,0:T(8,128)(2,1)} %param.21, bf16[2048,128]{1,0:T(8,128)(2,1)} %param.22, bf16[2048,4]{1,0:T(8,128)(2,1)S(1)} %copy.101, bf16[2048,4]{1,0:T(8,128)(2,1)S(1)} %copy.102), dimensions={1} | concatenate | bytes 6356992 | tf_op jit(solution)/shard_map/concatenate | solution.py:86
  24.2 12.3 %fusion.89 = (bf16[2048,776]{0,1:T(8,128)(2,1)S(1)}, f32[2048,776]{0,1:T(8,128)}) fusion(bf16[2048,776]{1,0:T(8,128)(2,1)} %concatenate.30, bf16[2048,2048]{1,0:T(8,128)(2,1)} %param.16, f32[2048]{0:T(1024)S(1)} %convert_element_type.94, f32[2048]{0:T(1024)S(1)} %add_rsqrt_fusion), kind=kOutput, calls=%fused_computation.134 | convolution fusion | flops 6527926272 | bytes 21118976 | tf_op jit(solution)/shard_map/dot_general | solution.py:98
  36.5 1.5 slice_convert_fusion.1
  38.0 0.5 copy.117
  38.5 1.3 split.36
  39.9 1.9 copy.135
  41.9 2.0 copy.134
  43.8 3.3 %subtract_convert_fusion = (bf16[2048,2,32]{2,0,1:T(8,128)(2,1)S(1)}, bf16[2048,2,32]{2,0,1:T(8,128)(2,1)S(1)}) fusion(f32[2048,2,32]{2,0,1:T(8,128)} %copy.135, f32[2048,2,32]{2,0,1:T(8,128)} %copy.134, f32[2048,32]{1,0:T(8,128)} %copy.116, f32[2048,32]{1,0:T(8,128)} %copy.114), kind=kLoop, calls=%fused_computation.45 | loop fusion | flops 1048576 | bytes 2097152 | tf_op jit(solution)/shard_map/convert.5
  47.2 1.1 copy-done.2
  48.2 2.0 fusion.107
  50.3 2.8 %split.55 = bf16[2048,256]{0,1:T(8,128)(2,1)} slice(f32[2048,776]{0,1:T(8,128)} %get-tuple-element.25), slice={[0:2048], [0:256]} | slice | bytes 2097152 | tf_op jit(solution)/shard_map/split | solution.py:115
  53.1 3.1 %split.34 = f32[2048,256]{0,1:T(8,128)} slice(f32[2048,776]{0,1:T(8,128)} %get-tuple-element.25), slice={[0:2048], [0:256]} | slice | bytes 4194304 | tf_op jit(solution)/shard_map/split | solution.py:115
  56.5 0.1 copy.133
  56.8 0.1 broadcast_in_dim.42
  57.0 0.1 broadcast_in_dim.43
  57.3 2.6 copy.103
  59.8 3.5 %reshape.279 = f32[64,32,2,64]{3,2,1,0:T(2,128)} reshape(f32[2048,128]{1,0:T(8,128)} %copy.103) | data formatting | bytes 2097152 | tf_op jit(solution)/shard_map/convert_element_type | solution.py:36
  63.3 2.8 %fusion.28 = bf16[2,64,32,64]{3,2,1,0:T(8,128)(2,1)} fusion(f32[64,32,2,64]{3,2,1,0:T(2,128)} %reshape.279, f32[2,32,64]{2,1,0:T(8,128)S(1)} %convert_element_type.101), kind=kLoop, calls=%fused_computation.42 | loop fusion | flops 524288 | bytes 1589248 | tf_op jit(solution)/shard_map/convert_element_type | solution.py:38
  66.1 2.7 reshape.269
  68.8 2.5 copy.105
  71.4 3.4 %reshape.280 = f32[64,32,2,64]{3,2,1,0:T(2,128)} reshape(f32[2048,128]{1,0:T(8,128)} %copy.105) | data formatting | bytes 2097152 | tf_op jit(solution)/shard_map/convert_element_type | solution.py:36
  74.8 2.8 %fusion.27 = bf16[2,64,32,64]{3,2,1,0:T(8,128)(2,1)} fusion(f32[64,32,2,64]{3,2,1,0:T(2,128)} %reshape.280, f32[2,32,64]{2,1,0:T(8,128)S(1)} %convert_element_type.108), kind=kLoop, calls=%fused_computation.40 | loop fusion | flops 524288 | bytes 1589248 | tf_op jit(solution)/shard_map/convert_element_type | solution.py:38
  77.5 15.1 %reshape.270 = bf16[2,64,2048]{2,1,0:T(8,128)(2,1)} reshape(bf16[2,64,32,64]{3,2,1,0:T(8,128)(2,1)} %fusion.27) | data formatting | bytes 1048576 | tf_op jit(solution)/shard_map/reshape | solution.py:39
  92.7 1.8 subtract_convert_fusion.1
  94.5 0.1 copy.136
  94.6 0.1 copy.111
  94.8 0.1 copy.137
  94.9 0.9 copy.112
  95.8 1.0 fusion.60
  96.8 1.6 mul.206
  98.3 3.7 %mul.207 = f32[4,512,256]{1,0,2:T(4,128)} reshape(f32[2048,4,64]{0,2,1:T(8,128)} %mul.206) | data formatting | bytes 4194304 | tf_op jit(solution)/shard_map/mul | solution.py:199
  102.0 3.2 %pad_maximum_fusion.1 = bf16[2048,2,128]{2,0,1:T(8,128)(2,1)} fusion(bf16[2048,2,64]{2,0,1:T(8,128)(2,1)S(1)} %copy.117, bf16[2048,2,32]{2,0,1:T(8,128)(2,1)} %copy-done.2, bf16[2048,2,32]{2,0,1:T(8,128)(2,1)S(1)} %get-tuple-element.7), kind=kLoop, calls=%fused_computation.54 | loop fusion | flops 3145728 | bytes 2097152 | tf_op jit(solution)/shard_map/concatenate | solution.py:156
  105.2 2.3 copy.121
  107.5 0.2 mul.224
  107.7 2.4 mul.225
  110.2 1.5 convolution_convert_fusion.2
  111.7 1.6 convolution_convert_fusion.1
  113.5 35.5 %all_gather.6 = bf16[2,512,128]{2,1,0:T(8,128)(2,1)S(1)} all-gather(bf16[2,64,128]{2,1,0:T(8,128)(2,1)S(1)} %pad_maximum_fusion.2), channel_id=1, replica_groups=mesh['kv'=8,'tp'=4] {'kv'}, dimensions={1}, use_global_device_ids=true | all-gather | bytes 294912 | tf_op jit(solution)/shard_map/all_gather | solution.py:134
  149.0 2.7 fusion.87
  151.7 9.7 %fusion.91 = (f32[2,2048,2]{1,2,0:T(2,128)S(1)}, f32[2,2048,2,512]{1,3,2,0:T(8,128)}) fusion(pred[2048,512]{0,1:T(8,128)(4,1)S(1)} %get-tuple-element.21, bf16[2,2048,2,64]{1,3,2,0:T(8,128)(2,1)S(1)} %bitcast.127, bf16[2,512,128]{2,1,0:T(8,128)(2,1)S(1)} %all_gather.6), kind=kOutput, calls=%fused_computation.136 | convolution fusion | flops 553648640 | bytes 19169280 | tf_op jit(solution)/shard_map/sub | solution.py:145
  161.4 8.2 %fusion.19 = f32[2048,2,2,64]{0,3,2,1:T(8,128)S(1)} fusion(f32[2,2048,2,512]{1,3,2,0:T(8,128)} %get-tuple-element.29, f32[2048,512]{0,1:T(8,128)} %get-tuple-element.20, f32[2,2048,2]{1,2,0:T(2,128)S(1)} %get-tuple-element.28, bf16[2,512,128]{2,1,0:T(8,128)(2,1)S(1)} %all_gather.6), kind=kOutput, calls=%fused_computation.32 | convolution fusion | flops 549453824 | bytes 23363584 | tf_op jit(solution)/shard_map/ktgc,kcd->ktgd/dot_general | solution.py:148
  169.6 2.4 reshape.271
  172.0 2.7 broadcast_compare_fusion
  174.7 7.8 %all-gather.2.cloned.1.call-done = bf16[2,16384,128]{2,1,0:T(8,128)(2,1)} async-done(((bf16[2,2048,128]{2,1,0:T(8,128)(2,1)}), bf16[2,16384,128]{2,1,0:T(8,128)(2,1)}) %all-gather.2.cloned.1.call-update) | async-done | bytes 8388624 | tf_op jit(solution)/shard_map/all_gather | solution.py:161
  182.5 6.7 %gather_fusion = bf16[256,64,128]{2,1,0:T(8,128)(2,1)} fusion(bf16[2,256,64,128]{3,2,1,0:T(8,128)(2,1)} %bitcast.123, s32[256]{0:T(256)S(1)} %reshape.281), kind=kCustom, calls=%fused_computation | custom fusion | bytes 8390656 | tf_op jit(solution)/shard_map/gather | solution.py:166
  189.2 6.3 %copy.120 = bf16[2,16,512,128]{2,3,1,0:T(8,128)(2,1)} copy(bf16[2,16,512,128]{3,2,1,0:T(8,128)(2,1)} %bitcast.117) | data formatting | bytes 8388608 | tf_op jit(solution)/shard_map/gather | solution.py:166
  195.5 2.6 broadcast_select_fusion
  198.2 8.6 %fusion.22 = f32[2,16,128,2,640]{4,2,3,1,0:T(8,128)} fusion(bf16[2,16,128,128]{2,3,1,0:T(8,128)(2,1)S(1)} %copy-done.3, bf16[2,16,512,128]{2,3,1,0:T(8,128)(2,1)S(1)} %broadcast_select_fusion, bf16[16,128,2,2,32]{1,4,3,0,2:T(8,128)(2,1)S(1)} %copy-done.5, bf16[16,128,2,2,32]{1,4,3,0,2:T(8,128)(2,1)S(1)} %copy.111), kind=kOutput, calls=%fused_computation.35 | convolution fusion | flops 678428672 | bytes 27262976 | tf_op jit(solution)/shard_map/knqgd,knmd->knqgm/dot_general | solution.py:184
  206.7 24.3 %fusion.90 = (f32[2,16,128,2]{2,3,1,0:T(2,128)S(1)}, f32[2,16,128,2,640]{4,2,3,1,0:T(8,128)}) fusion(f32[2,16,128,2,640]{4,2,3,1,0:T(8,128)} %fusion.22, pred[2,16,128,640]{3,2,1,0:T(8,128)(4,1)S(1)} %copy-done.4), kind=kOutput, calls=%fused_computation.135 | output fusion | flops 31457920 | bytes 44597248 | tf_op jit(solution)/shard_map/sub | solution.py:190
  231.1 9.1 %fusion.31 = f32[16,128,2,2,64]{1,4,3,0,2:T(8,128)S(1)} fusion(bf16[2,16,512,128]{2,3,1,0:T(8,128)(2,1)S(1)} %broadcast_select_fusion, bf16[2,16,128,128]{2,3,1,0:T(8,128)(2,1)S(1)} %copy-done.3, f32[2,16,128,2,640]{4,2,3,1,0:T(8,128)} %get-tuple-element.27, f32[2,16,128,2]{2,3,1,0:T(2,128)S(1)} %get-tuple-element.26), kind=kOutput, calls=%fused_computation.48 | convolution fusion | flops 686817280 | bytes 28344320 | tf_op jit(solution)/shard_map/knqgm,knmd->knqgd/dot_general | solution.py:191
  240.1 1.2 copy.122
  241.4 1.7 reshape.278
  243.1 4.5 %add_convert_fusion = bf16[4,512,256]{1,0,2:T(4,128)(2,1)S(1)} fusion(f32[4,512,256]{1,0,2:T(4,128)} %mul.225, f32[4,512,256]{1,0,2:T(4,128)} %reshape.278, f32[4,512,256]{1,0,2:T(4,128)} %mul.207, f32[4,512,256]{1,0,2:T(4,128)} %reshape.271), kind=kLoop, calls=%fused_computation.43 | loop fusion | flops 2097152 | bytes 9437184 | tf_op jit(solution)/shard_map/convert_element_type | solution.py:201
  247.7 0.2 copy.123
  247.9 17.2 %all_to_all.16 = bf16[4,512,256]{1,2,0:T(8,128)(2,1)S(1)} all-to-all(bf16[4,512,256]{1,2,0:T(8,128)(2,1)S(1)} %copy.123), channel_id=1, replica_groups=mesh['kv'=8,'tp'=4] {'tp'}, dimensions={0} | all-to-all | bytes 2097152 | tf_op jit(solution)/shard_map/all_to_all | solution.py:203
  265.1 3.8 %convolution_convert_fusion = bf16[512,2048]{1,0:T(8,128)(2,1)} fusion(bf16[512,1024]{0,1:T(8,128)(2,1)S(1)} %bitcast.128, bf16[1024,2048]{1,0:T(8,128)(2,1)S(1)} %copy-done.11), kind=kOutput, calls=%fused_computation.31 | convolution fusion | flops 2148532224 | bytes 7340032 | tf_op jit(solution)/shard_map/dot_general | solution.py:204
  (52 shorter events, 0.9 us)
Async XLA Ops:
  6.5 103.6 %copy-start = (bf16[2,2048,64]{1,2,0:T(8,128)(2,1)S(1)}, bf16[2,2048,64]{1,2,0:T(8,128)(2,1)}, u32[]{:S(2)}) copy-start(bf16[2,2048,64]{1,2,0:T(8,128)(2,1)} %param.25) | copy-start | bytes 1572868
  6.5 176.0 %all-gather.2.cloned.1.call-start = ((), (), s32[]{:S(2)}) async-start(), calls=%async_computation.1 | async-start | bytes 9437184 | tf_op jit(solution)/shard_map/all_gather | solution.py:161
  12.4 5.2 %copy-start.6 = (bf16[2048,256]{1,0:T(8,128)(2,1)S(1)}, bf16[2048,256]{1,0:T(8,128)(2,1)}, u32[]{:S(2)}) copy-start(bf16[2048,256]{1,0:T(8,128)(2,1)} %param.18) | copy-start | bytes 3145732
  47.2 1.1 copy-start.2
  50.2 6.1 %copy-start.8 = (bf16[2,32,64]{2,1,0:T(8,128)(2,1)S(1)}, bf16[2,32,64]{2,1,0:T(8,128)(2,1)}, u32[]{:S(2)}) copy-start(bf16[2,32,64]{2,1,0:T(8,128)(2,1)} %param.24) | copy-start | bytes 24580
  50.2 6.1 %copy-start.9 = (bf16[2,32,64]{2,1,0:T(8,128)(2,1)S(1)}, bf16[2,32,64]{2,1,0:T(8,128)(2,1)}, u32[]{:S(2)}) copy-start(bf16[2,32,64]{2,1,0:T(8,128)(2,1)} %param.27) | copy-start | bytes 24580
  50.2 6.1 %copy-start.10 = (s32[2,128,8]{1,2,0:T(8,128)S(1)}, s32[2,128,8]{1,2,0:T(8,128)}, u32[]{:S(2)}) copy-start(s32[2,128,8]{1,2,0:T(8,128)} %param.31) | copy-start | bytes 24580
  105.2 5.0 %copy-start.12 = (bf16[2,64,64]{2,1,0:T(8,128)(2,1)S(1)}, bf16[2,64,64]{2,1,0:T(8,128)(2,1)}, u32[]{:S(2)}) copy-start(bf16[2,64,64]{2,1,0:T(8,128)(2,1)} %param.26) | copy-start | bytes 49156
  107.5 4.2 %copy-start.13 = (bf16[2,64,64]{2,1,0:T(8,128)(2,1)S(1)}, bf16[2,64,64]{2,1,0:T(8,128)(2,1)}, u32[]{:S(2)}) copy-start(bf16[2,64,64]{2,1,0:T(8,128)(2,1)} %param.29) | copy-start | bytes 49156
  110.2 41.6 %copy-start.7 = (bf16[2048,256]{0,1:T(8,128)(2,1)S(1)}, bf16[2048,256]{0,1:T(8,128)(2,1)}, u32[]{:S(2)}) copy-start(bf16[2048,256]{0,1:T(8,128)(2,1)} %split.55) | copy-start | bytes 3145732
  195.5 2.6 copy-start.3
  195.5 2.7 copy-start.5
  198.2 8.6 %copy-start.4 = (pred[2,16,128,640]{3,2,1,0:T(8,128)(4,1)S(1)}, pred[2,16,128,640]{3,2,1,0:T(8,128)(4,1)}, u32[]{:S(2)}) copy-start(pred[2,16,128,640]{3,2,1,0:T(8,128)(4,1)} %broadcast_compare_fusion) | copy-start | bytes 7864324
  247.6 17.5 %copy-start.11 = (bf16[1024,2048]{1,0:T(8,128)(2,1)S(1)}, bf16[1024,2048]{1,0:T(8,128)(2,1)}, u32[]{:S(2)}) copy-start(bf16[1024,2048]{1,0:T(8,128)(2,1)} %param.30) | copy-start | bytes 12582916
  265.1 3.8 %copy-start.1 = (bf16[2,2048,64]{1,2,0:T(8,128)(2,1)S(1)}, bf16[2,2048,64]{1,2,0:T(8,128)(2,1)}, u32[]{:S(2)}) copy-start(bf16[2,2048,64]{1,2,0:T(8,128)(2,1)} %param.25) | copy-start | bytes 1572868
Sparse Core Ops, SparseCore 0:
  50.4 132.0 all-gather.1
where the time goes:
time: 280 us; the launch traced here: 276 us
  local copies, waits for them, and re-layouts  84.3 us (30%)
  other arithmetic  62.4 us (22%)
  matrix products  54.7 us (20%)
  blocking collectives  52.8 us (19%)
  between operations  13.9 us (5%)
  waiting for transfers between devices  7.81 us (3%)
    all_gather x1, blocking collectives, per_device(): summaries = lax.all_gather(summary, 'kv', axis=1, tiled=True)  35.5 us
    sub x1, other arithmetic, per_device(): jax.nn.softmax(jnp.where(allowed_keys, sel_scores, masked_score), axis=-1)  24.3 us
    reshape x2, local copies, waits for them, and re-layouts, summarize(): blocked = blocked.reshape(kv_local, block_count, CMP_BLOCK * HEAD_DIM)  17.8 us
    all_to_all x1, blocking collectives, per_device(): lax.all_to_all(mixed, 'tp', split_axis=0, concat_axis=1, tiled=True)  17.2 us
    gather x2, local copies, waits for them, and re-layouts, per_device(): fetched = blocked[head_lane, clipped]  13 us
    dot_general x1, matrix products, per_device(): jnp.dot(normed, joined_weight, preferred_element_type=jnp.float32)  12.3 us
    convert_element_type x4, local copies, waits for them, and re-layouts, summarize(): blocked = raw_rows.reshape(block_count, CMP_BLOCK, kv_local, HEAD_DIM).tr...  12 us
    sub x1, matrix products, per_device(): jax.nn.softmax(jnp.where(usable, cmp_scores, masked_score), axis=-1)  9.68 us
  transfers between devices with their start and end apart: 1, of which 1 were waited for; matrix products, arithmetic and copies ran while one was open for 32% of the time, Pallas kernels for 0%

commit v1 on v0

--- a/solution.py
+++ b/solution.py
@@ -200,7 +200,9 @@
         .reshape(tok_rows, heads_local * HEAD_DIM)
         .astype(jnp.bfloat16)
     )
-    head_rows = lax.all_to_all(mixed, "tp", split_axis=0, concat_axis=1, tiled=True)
+    head_rows = jnp.concatenate(
+        lax.all_to_all(jnp.stack(jnp.split(mixed, lax.axis_size("tp"), axis=0)), "tp", 0, 0), axis=1
+    )
     return jnp.dot(head_rows, out_weight, preferred_element_type=jnp.float32).astype(jnp.bfloat16)
 
 

time: 280 us -> 269 us (0.961); the launches traced: 276 us -> 268 us
  local copies, waits for them, and re-layouts: 84.3 us -> 59.1 us
  waiting for transfers between devices: 7.81 us -> 28.7 us
  other arithmetic: 62.4 us -> 57.7 us
    all_gather x1, waiting for transfers between devices: 7.79 us -> 28.7 us  [per_device(): piece = lax.all_gather(kv_sel, 'kv', axis=1, tiled=True)]
    reshape x2, local copies, waits for them, and re-layouts: 17.8 us -> 5.43 us  [summarize(): blocked = blocked.reshape(kv_local, block_count, CMP_BLOCK * HEAD_DIM)]
    mul x4 -> x0, local copies, waits for them, and re-layouts: 7.9 us -> none  [the longest x2 5.26 us: per_device(): gate_cmp[..., None] * out_cmp + gate_sel[..., None] * out_sel]
    reshape x2 -> x0, local copies, waits for them, and re-layouts: 4.14 us -> none  [the longest x1 2.4 us: per_device(): out_cmp.transpose(1, 0, 2, 3).reshape(tok_rows, heads_local, HEAD_DIM)]
    convert_element_type x1, other arithmetic: 4.54 us -> 0.98 us  [per_device(): mixed = (gate_cmp[..., None] * out_cmp + gate_sel[..., None] * out_sel).r...]
  transfers between devices with their start and end apart: 1 -> 1, of which waited for: 1 -> 1; matrix products, arithmetic and copies ran while one was open for 32% -> 25% of each run, Pallas kernels for 0% -> 0%
where the time goes in v1:
time: 269 us; the launch traced here: 268 us
  local copies, waits for them, and re-layouts  59.1 us (22%)
  other arithmetic  57.7 us (21%)
  matrix products  57.4 us (21%)
  blocking collectives  51.5 us (19%)
  waiting for transfers between devices  28.7 us (11%)
  between operations  13.7 us (5%)
    all_gather x1, blocking collectives, per_device(): summaries = lax.all_gather(summary, 'kv', axis=1, tiled=True)  34.3 us
    all_gather x1, waiting for transfers between devices, per_device(): piece = lax.all_gather(kv_sel, 'kv', axis=1, tiled=True)  28.7 us
    sub x1, other arithmetic, per_device(): jax.nn.softmax(jnp.where(allowed_keys, sel_scores, masked_score), axis=-1)  24.3 us
    all_to_all x1, blocking collectives, per_device(): lax.all_to_all(jnp.stack(jnp.split(mixed, lax.axis_size('tp'), axis=0)),...  17.2 us
    gather x2, local copies, waits for them, and re-layouts, per_device(): fetched = blocked[head_lane, clipped]  13 us
    dot_general x1, matrix products, per_device(): jnp.dot(normed, joined_weight, preferred_element_type=jnp.float32)  12.4 us
    convert_element_type x4, local copies, waits for them, and re-layouts, summarize(): blocked = raw_rows.reshape(block_count, CMP_BLOCK, kv_local, HEAD_DIM).tr...  12 us
    sub x1, matrix products, per_device(): jax.nn.softmax(jnp.where(usable, cmp_scores, masked_score), axis=-1)  10.7 us
  transfers between devices with their start and end apart: 1, of which 1 were waited for; matrix products, arithmetic and copies ran while one was open for 25% of the time, Pallas kernels for 0%

profile of v1, /device:TPU:0, one launch (start us, length us, event | category | flops | bytes accessed | tf_op | source)
XLA Modules:
  0.0 268.1 jit_solution(14101893366955559044)
XLA Ops:
  6.6 0.7 convert_element_type.93
  7.3 5.1 %fusion.2 = f32[2048]{0:T(1024)S(1)} fusion(bf16[2048,2048]{1,0:T(8,128)(2,1)} %param.16), kind=kLoop, calls=%fused_computation.8 | loop fusion | flops 12580864 | bytes 8396800 | tf_op jit(solution)/shard_map/reduce_sum | solution.py:78
  12.4 0.9 dynamic-slice_bitcast_fusion
  13.3 0.3 copy.75
  13.6 0.3 copy.74
  13.9 1.0 multiply_cosine_fusion
  14.9 1.3 copy.87
  16.2 1.3 copy.89
  17.5 6.3 %concatenate.30 = bf16[2048,776]{1,0:T(8,128)(2,1)} concatenate(bf16[2048,256]{1,0:T(8,128)(2,1)S(1)} %copy-done.7, bf16[2048,128]{1,0:T(8,128)(2,1)} %param.19, bf16[2048,128]{1,0:T(8,128)(2,1)} %param.20, bf16[2048,128]{1,0:T(8,128)(2,1)} %param.21, bf16[2048,128]{1,0:T(8,128)(2,1)} %param.22, bf16[2048,4]{1,0:T(8,128)(2,1)S(1)} %copy.74, bf16[2048,4]{1,0:T(8,128)(2,1)S(1)} %copy.75), dimensions={1} | concatenate | bytes 6356992 | tf_op jit(solution)/shard_map/concatenate | solution.py:86
  23.8 12.4 %fusion.90 = (bf16[2048,776]{0,1:T(8,128)(2,1)S(1)}, f32[2048,776]{0,1:T(8,128)}) fusion(bf16[2048,776]{1,0:T(8,128)(2,1)} %concatenate.30, bf16[2048,2048]{1,0:T(8,128)(2,1)} %param.16, f32[2048]{0:T(1024)S(1)} %convert_element_type.93, f32[2048]{0:T(1024)S(1)} %add_rsqrt_fusion), kind=kOutput, calls=%fused_computation.141 | convolution fusion | flops 6527926272 | bytes 21118976 | tf_op jit(solution)/shard_map/dot_general | solution.py:98
  36.2 1.5 slice_convert_fusion.1
  37.8 0.5 copy.90
  38.2 1.3 split.52
  39.7 1.9 copy.107
  41.6 2.0 copy.106
  43.5 3.3 %subtract_convert_fusion = (bf16[2048,2,32]{2,0,1:T(8,128)(2,1)S(1)}, bf16[2048,2,32]{2,0,1:T(8,128)(2,1)S(1)}) fusion(f32[2048,2,32]{2,0,1:T(8,128)} %copy.107, f32[2048,2,32]{2,0,1:T(8,128)} %copy.106, f32[2048,32]{1,0:T(8,128)} %copy.89, f32[2048,32]{1,0:T(8,128)} %copy.87), kind=kLoop, calls=%fused_computation.47 | loop fusion | flops 1048576 | bytes 2097152 | tf_op jit(solution)/shard_map/convert.5
  46.9 1.0 copy-done.2
  47.9 1.9 fusion.108
  49.9 2.8 %split.79 = bf16[2048,256]{0,1:T(8,128)(2,1)} slice(f32[2048,776]{0,1:T(8,128)} %get-tuple-element.29), slice={[0:2048], [0:256]} | slice | bytes 2097152 | tf_op jit(solution)/shard_map/split | solution.py:115
  52.7 3.1 %split.50 = f32[2048,256]{0,1:T(8,128)} slice(f32[2048,776]{0,1:T(8,128)} %get-tuple-element.29), slice={[0:2048], [0:256]} | slice | bytes 4194304 | tf_op jit(solution)/shard_map/split | solution.py:115
  55.8 0.1 add.160
  56.1 0.1 copy.105
  56.3 0.1 reshape.282
  56.5 0.1 broadcast_in_dim.42
  56.6 0.1 broadcast_in_dim.43
  56.7 0.1 add.157
  56.8 0.1 add.158
  56.9 2.6 copy.76
  59.5 3.5 %reshape.280 = f32[64,32,2,64]{3,2,1,0:T(2,128)} reshape(f32[2048,128]{1,0:T(8,128)} %copy.76) | data formatting | bytes 2097152 | tf_op jit(solution)/shard_map/convert_element_type | solution.py:36
  62.9 2.8 %fusion.29 = bf16[2,64,32,64]{3,2,1,0:T(8,128)(2,1)} fusion(f32[64,32,2,64]{3,2,1,0:T(2,128)} %reshape.280, f32[2,32,64]{2,1,0:T(8,128)S(1)} %convert_element_type.100), kind=kLoop, calls=%fused_computation.45 | loop fusion | flops 524288 | bytes 1589248 | tf_op jit(solution)/shard_map/convert_element_type | solution.py:38
  65.7 2.7 %reshape.268 = bf16[2,64,2048]{2,1,0:T(8,128)(2,1)} reshape(bf16[2,64,32,64]{3,2,1,0:T(8,128)(2,1)} %fusion.29) | data formatting | bytes 1048576 | tf_op jit(solution)/shard_map/reshape | solution.py:39
  68.4 2.5 copy.78
  71.0 3.4 %reshape.281 = f32[64,32,2,64]{3,2,1,0:T(2,128)} reshape(f32[2048,128]{1,0:T(8,128)} %copy.78) | data formatting | bytes 2097152 | tf_op jit(solution)/shard_map/convert_element_type | solution.py:36
  74.4 2.8 %fusion.28 = bf16[2,64,32,64]{3,2,1,0:T(8,128)(2,1)} fusion(f32[64,32,2,64]{3,2,1,0:T(2,128)} %reshape.281, f32[2,32,64]{2,1,0:T(8,128)S(1)} %convert_element_type.107), kind=kLoop, calls=%fused_computation.43 | loop fusion | flops 524288 | bytes 1589248 | tf_op jit(solution)/shard_map/convert_element_type | solution.py:38
  77.1 2.7 %reshape.269 = bf16[2,64,2048]{2,1,0:T(8,128)(2,1)} reshape(bf16[2,64,32,64]{3,2,1,0:T(8,128)(2,1)} %fusion.28) | data formatting | bytes 1048576 | tf_op jit(solution)/shard_map/reshape | solution.py:39
  79.9 1.9 subtract_convert_fusion.1
  81.8 0.1 copy.108
  81.9 0.1 copy.84
  82.1 0.1 copy.109
  82.2 1.0 copy.85
  83.2 1.9 pad_maximum_fusion.1
  85.1 1.6 copy.94
  86.8 1.5 convolution_convert_fusion.2
  88.2 1.6 convolution_convert_fusion.1
  89.9 0.1 pad_maximum_fusion.3
  90.0 34.3 %all_gather.6 = bf16[2,512,128]{2,1,0:T(8,128)(2,1)S(1)} all-gather(bf16[2,64,128]{2,1,0:T(8,128)(2,1)S(1)} %pad_maximum_fusion.3), channel_id=1, replica_groups=mesh['kv'=8,'tp'=4] {'kv'}, dimensions={1}, use_global_device_ids=true | all-gather | bytes 294912 | tf_op jit(solution)/shard_map/all_gather | solution.py:134
  124.3 1.0 fusion.61
  125.3 2.7 %broadcast_compare_fusion = pred[2,16,128,640]{3,2,1,0:T(8,128)(4,1)} fusion(s32[16,128]{1,0:T(8,128)S(1)} %add_add_fusion, s32[2,16,640]{2,1,0:T(8,128)S(1)} %pad_add_fusion), kind=kLoop, calls=%fused_computation.29 | loop fusion | flops 2621440 | bytes 2711552 | tf_op jit(solution)/shard_map/le | solution.py:189
  128.0 2.8 %fusion.88 = (f32[2048,512]{0,1:T(8,128)}, pred[2048,512]{0,1:T(8,128)(4,1)S(1)}) fusion(s32[2048]{0:T(1024)S(1)} %get-tuple-element.34, s32[512]{0:T(512)S(1)} %multiply_add_fusion), kind=kLoop, calls=%fused_computation.139 | loop fusion | flops 2097152 | bytes 5253120 | tf_op jit(solution)/shard_map/convert_element_type | solution.py:147
  130.7 10.7 %fusion.92 = (f32[2,2048,2]{1,2,0:T(2,128)S(1)}, f32[2,2048,2,512]{1,3,2,0:T(8,128)}) fusion(pred[2048,512]{0,1:T(8,128)(4,1)S(1)} %get-tuple-element.25, bf16[2,2048,2,64]{1,3,2,0:T(8,128)(2,1)} %bitcast.142, bf16[2,512,128]{2,1,0:T(8,128)(2,1)S(1)} %all_gather.6), kind=kOutput, calls=%fused_computation.143 | convolution fusion | flops 553648640 | bytes 19169280 | tf_op jit(solution)/shard_map/sub | solution.py:145
  141.4 9.7 %fusion.18 = f32[2,2048,2,64]{1,3,2,0:T(8,128)} fusion(f32[2,2048,2,512]{1,3,2,0:T(8,128)} %get-tuple-element.33, f32[2048,512]{0,1:T(8,128)} %get-tuple-element.24, f32[2,2048,2]{1,2,0:T(2,128)S(1)} %get-tuple-element.32, bf16[2,512,128]{2,1,0:T(8,128)(2,1)S(1)} %all_gather.6), kind=kOutput, calls=%fused_computation.26 | convolution fusion | flops 549453824 | bytes 23363584 | tf_op jit(solution)/shard_map/ktgc,kcd->ktgd/dot_general | solution.py:148
  151.2 28.7 %all-gather.2.cloned.1.call-done = bf16[2,16384,128]{2,1,0:T(8,128)(2,1)} async-done(((bf16[2,2048,128]{2,1,0:T(8,128)(2,1)}), bf16[2,16384,128]{2,1,0:T(8,128)(2,1)}) %all-gather.2.cloned.1.call-update) | async-done | bytes 8388624 | tf_op jit(solution)/shard_map/all_gather | solution.py:161
  179.9 6.7 %gather_fusion = bf16[256,64,128]{2,1,0:T(8,128)(2,1)} fusion(bf16[2,256,64,128]{3,2,1,0:T(8,128)(2,1)} %bitcast.138, s32[256]{0:T(256)S(1)} %reshape.282), kind=kCustom, calls=%fused_computation | custom fusion | bytes 8390656 | tf_op jit(solution)/shard_map/gather | solution.py:166
  186.6 6.3 %copy.93 = bf16[2,16,512,128]{2,3,1,0:T(8,128)(2,1)} copy(bf16[2,16,512,128]{3,2,1,0:T(8,128)(2,1)} %bitcast.131) | data formatting | bytes 8388608 | tf_op jit(solution)/shard_map/gather | solution.py:166
  192.9 2.6 broadcast_select_fusion
  195.5 8.6 %fusion.21 = f32[2,16,128,2,640]{4,2,3,1,0:T(8,128)} fusion(bf16[2,16,128,128]{2,3,1,0:T(8,128)(2,1)S(1)} %copy.94, bf16[2,16,512,128]{2,3,1,0:T(8,128)(2,1)S(1)} %broadcast_select_fusion, bf16[16,128,2,2,32]{1,4,3,0,2:T(8,128)(2,1)S(1)} %copy-done.6, bf16[16,128,2,2,32]{1,4,3,0,2:T(8,128)(2,1)S(1)} %copy.84), kind=kOutput, calls=%fused_computation.34 | convolution fusion | flops 678428672 | bytes 27262976 | tf_op jit(solution)/shard_map/knqgd,knmd->knqgm/dot_general | solution.py:184
  204.0 24.3 %fusion.91 = (f32[2,16,128,2]{2,3,1,0:T(2,128)S(1)}, f32[2,16,128,2,640]{4,2,3,1,0:T(8,128)}) fusion(f32[2,16,128,2,640]{4,2,3,1,0:T(8,128)} %fusion.21, pred[2,16,128,640]{3,2,1,0:T(8,128)(4,1)S(1)} %copy-done.4), kind=kOutput, calls=%fused_computation.142 | output fusion | flops 31457920 | bytes 44597248 | tf_op jit(solution)/shard_map/sub | solution.py:190
  228.4 9.1 %fusion.32 = f32[16,128,2,2,64]{1,4,3,0,2:T(8,128)S(1)} fusion(bf16[2,16,512,128]{2,3,1,0:T(8,128)(2,1)S(1)} %broadcast_select_fusion, bf16[2,16,128,128]{2,3,1,0:T(8,128)(2,1)S(1)} %copy.94, f32[2,16,128,2,640]{4,2,3,1,0:T(8,128)} %get-tuple-element.31, f32[2,16,128,2]{2,3,1,0:T(2,128)S(1)} %get-tuple-element.30), kind=kOutput, calls=%fused_computation.50 | convolution fusion | flops 686817280 | bytes 28344320 | tf_op jit(solution)/shard_map/knqgm,knmd->knqgd/dot_general | solution.py:191
  237.5 1.2 copy.95
  238.7 0.4 copy-done.5
  239.1 1.0 fusion.27
  240.2 0.1 pad_maximum_fusion.2
  240.3 17.2 %all_to_all.5 = bf16[4,512,256]{1,2,0:T(8,128)(2,1)S(1)} all-to-all(bf16[4,512,256]{1,2,0:T(8,128)(2,1)S(1)} %pad_maximum_fusion.2), channel_id=1, replica_groups=mesh['kv'=8,'tp'=4] {'tp'}, dimensions={0} | all-to-all | bytes 2097152 | tf_op jit(solution)/shard_map/all_to_all | solution.py:204
  257.5 3.8 %convolution_convert_fusion = bf16[512,2048]{1,0:T(8,128)(2,1)} fusion(bf16[512,1024]{0,1:T(8,128)(2,1)S(1)} %bitcast.143, bf16[1024,2048]{1,0:T(8,128)(2,1)S(1)} %copy-done.11), kind=kOutput, calls=%fused_computation.31 | convolution fusion | flops 2148532224 | bytes 7340032 | tf_op jit(solution)/shard_map/dot_general | solution.py:206
  (47 shorter events, 0.6 us)
Async XLA Ops:
  6.5 80.2 %copy-start = (bf16[2,2048,64]{1,2,0:T(8,128)(2,1)S(1)}, bf16[2,2048,64]{1,2,0:T(8,128)(2,1)}, u32[]{:S(2)}) copy-start(bf16[2,2048,64]{1,2,0:T(8,128)(2,1)} %param.25) | copy-start | bytes 1572868
  6.5 173.3 %all-gather.2.cloned.1.call-start = ((), (), s32[]{:S(2)}) async-start(), calls=%async_computation.1 | async-start | bytes 9437184 | tf_op jit(solution)/shard_map/all_gather | solution.py:161
  12.4 5.2 %copy-start.7 = (bf16[2048,256]{1,0:T(8,128)(2,1)S(1)}, bf16[2048,256]{1,0:T(8,128)(2,1)}, u32[]{:S(2)}) copy-start(bf16[2048,256]{1,0:T(8,128)(2,1)} %param.18) | copy-start | bytes 3145732
  46.9 1.1 copy-start.2
  49.9 6.0 %copy-start.8 = (bf16[2,32,64]{2,1,0:T(8,128)(2,1)S(1)}, bf16[2,32,64]{2,1,0:T(8,128)(2,1)}, u32[]{:S(2)}) copy-start(bf16[2,32,64]{2,1,0:T(8,128)(2,1)} %param.24) | copy-start | bytes 24580
  49.9 6.0 %copy-start.9 = (bf16[2,32,64]{2,1,0:T(8,128)(2,1)S(1)}, bf16[2,32,64]{2,1,0:T(8,128)(2,1)}, u32[]{:S(2)}) copy-start(bf16[2,32,64]{2,1,0:T(8,128)(2,1)} %param.27) | copy-start | bytes 24580
  49.9 6.0 %copy-start.10 = (s32[2,128,8]{1,2,0:T(8,128)S(1)}, s32[2,128,8]{1,2,0:T(8,128)}, u32[]{:S(2)}) copy-start(s32[2,128,8]{1,2,0:T(8,128)} %param.31) | copy-start | bytes 24580
  79.9 3.3 %copy-start.3 = (bf16[2048,2,32]{2,0,1:T(8,128)(2,1)S(1)}, bf16[2048,2,32]{2,0,1:T(8,128)(2,1)}, u32[]{:S(2)}) copy-start(bf16[2048,2,32]{2,0,1:T(8,128)(2,1)} %copy-done.2) | copy-start | bytes 786436
  82.1 4.7 %copy-start.12 = (bf16[2,64,64]{2,1,0:T(8,128)(2,1)S(1)}, bf16[2,64,64]{2,1,0:T(8,128)(2,1)}, u32[]{:S(2)}) copy-start(bf16[2,64,64]{2,1,0:T(8,128)(2,1)} %param.26) | copy-start | bytes 49156
  82.2 6.0 %copy-start.13 = (bf16[2,64,64]{2,1,0:T(8,128)(2,1)S(1)}, bf16[2,64,64]{2,1,0:T(8,128)(2,1)}, u32[]{:S(2)}) copy-start(bf16[2,64,64]{2,1,0:T(8,128)(2,1)} %param.29) | copy-start | bytes 49156
  192.9 2.6 copy-start.6
  195.5 8.6 %copy-start.4 = (pred[2,16,128,640]{3,2,1,0:T(8,128)(4,1)S(1)}, pred[2,16,128,640]{3,2,1,0:T(8,128)(4,1)}, u32[]{:S(2)}) copy-start(pred[2,16,128,640]{3,2,1,0:T(8,128)(4,1)} %broadcast_compare_fusion) | copy-start | bytes 7864324
  237.5 1.6 copy-start.5
  240.1 17.4 %copy-start.11 = (bf16[1024,2048]{1,0:T(8,128)(2,1)S(1)}, bf16[1024,2048]{1,0:T(8,128)(2,1)}, u32[]{:S(2)}) copy-start(bf16[1024,2048]{1,0:T(8,128)(2,1)} %param.30) | copy-start | bytes 12582916
  257.5 3.8 %copy-start.1 = (bf16[2,2048,64]{1,2,0:T(8,128)(2,1)S(1)}, bf16[2,2048,64]{1,2,0:T(8,128)(2,1)}, u32[]{:S(2)}) copy-start(bf16[2,2048,64]{1,2,0:T(8,128)(2,1)} %param.25) | copy-start | bytes 1572868
Sparse Core Ops, SparseCore 0:
  50.1 129.7 all-gather.1
